TPU v7x, 32 devices: a whole 2x2x4 slice. The times are simulated.
32 devices in a mesh: sp: 8 (over z, y), tp: 4 (over x, core).
Axes of the slice: x: 2, y: 2, z: 4, core: 2. Of those that a mesh axis runs over, the one named last changes fastest.
Arguments:
- latent: bfloat16 [4096, 2048], P(('sp', 'tp')), may hold values from -6 to 6
- context: bfloat16 [512, 2048], P('sp'), may hold values from -6 to 6
- condition: float32 [2048], replicated, may hold values from -6 to 6
- context_condition: float32 [2048], replicated, may hold values from -6 to 6
- norm_gain: float32 [2048], replicated, may hold values from 0.1 to 1.9
- shift_weight: bfloat16 [2048, 2048], P('sp', 'tp'), may hold values from -0.21875 to 0.21875
- scale_weight: bfloat16 [2048, 2048], P('sp', 'tp'), may hold values from -0.21875 to 0.21875
- gate_weight: bfloat16 [2048, 2048], P('sp', 'tp'), may hold values from -0.21875 to 0.21875
- query_weight: bfloat16 [2048, 1024], P(None, 'tp'), may hold values from -1 to 1
- key_weight: bfloat16 [2048, 512], P(None, 'tp'), may hold values from -1 to 1
- value_weight: bfloat16 [2048, 512], P(None, 'tp'), may hold values from -0.125 to 0.125
- query_gain: float32 [64], replicated, may hold values from 0.1 to 7.8
- key_gain: float32 [64], replicated, may hold values from 0.1 to 7.8
- output_weight: bfloat16 [1024, 2048], replicated, may hold values from -1 to 1
Outputs:
- updated: bfloat16 [4096, 2048], P(('sp', 'tp'))
All inputs are finite; a program needn't handle non-finite values.
Results may differ from a plain program's by a relative error of at most 0.012.
The roundings to bfloat16 on the way count: a program that leaves them out, or rounds other values in their place, can miss the bound.
Values may be sent and summed in bfloat16 or wider, within the bound.
A program may use at most 64 MiB of HBM per device.

v0:
```python
import math

import jax
import jax.numpy as jnp
from jax import lax
from jax.sharding import PartitionSpec as P

CHANNEL_SPAN = 64
GRID_W = 64


epsilon = 1e-06
rope_base = 10000.0


def modulate(tok_rows, norm_gain, shift_row, scale_row):
    wide = tok_rows.astype(jnp.float32)
    normed = wide * lax.rsqrt(jnp.mean(wide * wide, axis=-1, keepdims=True) + epsilon)
    return (normed * norm_gain * (1.0 + scale_row) + shift_row).astype(jnp.bfloat16)


def headnorm(raw, gain, heads):
    field = raw.reshape(raw.shape[0], heads, -1)
    return field * lax.rsqrt(jnp.mean(field * field, axis=-1, keepdims=True) + epsilon) * gain


def rotate(field, places):
    count = field.shape[0]
    heads = field.shape[1]
    quarter = field.shape[2] // 4
    grid_row = (places // GRID_W).astype(jnp.float32)
    grid_col = (places % GRID_W).astype(jnp.float32)
    inverse = rope_base ** (-jnp.arange(quarter, dtype=jnp.float32) / quarter)
    angles = jnp.stack([grid_row[:, None] * inverse, grid_col[:, None] * inverse], axis=1)[:, None]
    cosine = jnp.cos(angles)
    sine = jnp.sin(angles)
    matcher_content_couples = field.reshape(count, heads, 2, 2, quarter)
    first = matcher_content_couples[:, :, :, 0]
    second = matcher_content_couples[:, :, :, 1]
    turned = jnp.stack([first * cosine - second * sine, second * cosine + first * sine], axis=3)
    return turned.reshape(count, heads, 4 * quarter)


def process_probe_group(
    accumulator_carry, probe_entries, matcher_content_couples, similarity_offset
):
    row_peak, row_total, weighted = accumulator_carry
    kv_heads = probe_entries.shape[1]
    head_size = probe_entries.shape[3]
    pair_width = kv_heads * head_size
    matcher_pieces = matcher_content_couples[:, :pair_width].reshape(
        matcher_content_couples.shape[0], kv_heads, head_size
    )
    value_rows = matcher_content_couples[:, pair_width:].reshape(
        matcher_content_couples.shape[0], kv_heads, head_size
    )
    similarity_matrix = (
        jnp.einsum(
            "dmvk,hmk->dmvh", probe_entries, matcher_pieces, preferred_element_type=jnp.float32
        )
        * head_size ** (-0.5)
        + similarity_offset
    )
    new_peak = jnp.maximum(row_peak, jnp.max(similarity_matrix, axis=-1))
    shares = jnp.exp(similarity_matrix - new_peak[..., None])
    shrink = jnp.exp(row_peak - new_peak)
    row_total = row_total * shrink + jnp.sum(shares, axis=-1)
    weighted = weighted * shrink[..., None] + jnp.einsum(
        "qkgn,nkd->qkgd",
        shares.astype(jnp.bfloat16),
        value_rows,
        preferred_element_type=jnp.float32,
    )
    return (new_peak, row_total, weighted)


def group_walker(accumulator_carry, probe_entries, matcher_content_couples, similarity_offset):
    pair_count = matcher_content_couples.shape[0]
    probe_group_total = -(-pair_count // 2048)
    while pair_count % probe_group_total:
        probe_group_total += 1
    if probe_group_total == 1:
        return process_probe_group(
            accumulator_carry, probe_entries, matcher_content_couples, similarity_offset
        )
    group_extent = pair_count // probe_group_total

    def scan_step(inner, slices):
        return (process_probe_group(inner, probe_entries, slices[0], slices[1]), None)

    result, unused = lax.scan(
        scan_step,
        accumulator_carry,
        (
            matcher_content_couples.reshape(
                probe_group_total, group_extent, matcher_content_couples.shape[1]
            ),
            similarity_offset.reshape(probe_group_total, group_extent),
        ),
    )
    return result


def on_device(
    latent,
    context,
    condition,
    context_condition,
    norm_gain,
    shift_weight,
    scale_weight,
    gate_weight,
    query_weight,
    key_weight,
    value_weight,
    query_gain,
    key_gain,
    output_weight,
):
    head_split = lax.axis_size("tp")
    seq_index = lax.axis_index("sp")
    head_index = lax.axis_index("tp")
    row_slab = shift_weight.shape[0]
    columns = shift_weight.shape[1]
    conditions = jnp.stack([condition, context_condition])
    activated = jax.nn.silu(
        lax.dynamic_slice_in_dim(conditions, seq_index * row_slab, row_slab, 1)
    ).astype(jnp.bfloat16)
    part_shift = jnp.dot(activated, shift_weight, preferred_element_type=jnp.float32)
    part_scale = jnp.dot(activated, scale_weight, preferred_element_type=jnp.float32)
    part_gate = jnp.dot(activated, gate_weight, preferred_element_type=jnp.float32)

    def widen(member):
        blank = jnp.zeros((2, columns * head_split), jnp.float32)
        return lax.dynamic_update_slice_in_dim(blank, member, head_index * columns, 1)

    shifts, scales, gates = lax.psum(
        (widen(part_shift), widen(part_scale), widen(part_gate)), ("sp", "tp")
    )
    own_rows = latent.shape[0]
    tok_count = own_rows * head_split
    ctx_rows = context.shape[0]
    hidden = modulate(latent, norm_gain, shifts[0], scales[0])
    context_hidden = modulate(context, norm_gain, shifts[1], scales[1])
    q_heads = query_weight.shape[1] // CHANNEL_SPAN
    kv_heads = key_weight.shape[1] // CHANNEL_SPAN
    group_size = q_heads // kv_heads
    q_width = q_heads * CHANNEL_SPAN
    kv_width = kv_heads * CHANNEL_SPAN
    joined_weight = jnp.concatenate([query_weight, key_weight, value_weight], axis=1)
    projected = jnp.dot(
        lax.all_gather(hidden, "tp", axis=0, tiled=True),
        joined_weight,
        preferred_element_type=jnp.float32,
    )
    places = seq_index * tok_count + jnp.arange(tok_count, dtype=jnp.int32)
    probe_entries = rotate(headnorm(projected[:, :q_width], query_gain, q_heads), places).astype(
        jnp.bfloat16
    )
    probe_entries = probe_entries.reshape(tok_count, kv_heads, group_size, CHANNEL_SPAN)
    latent_keys = rotate(
        headnorm(projected[:, q_width : q_width + kv_width], key_gain, kv_heads), places
    ).astype(jnp.bfloat16)
    latent_values = projected[:, q_width + kv_width :].astype(jnp.bfloat16)
    own_pairs = jnp.concatenate([latent_keys.reshape(tok_count, kv_width), latent_values], axis=1)
    ctx_projected = jnp.dot(
        context_hidden, joined_weight[:, q_width:], preferred_element_type=jnp.float32
    )
    ctx_keys = (
        headnorm(ctx_projected[:, :kv_width], key_gain, kv_heads)
        .astype(jnp.bfloat16)
        .reshape(ctx_rows, kv_width)
    )
    ctx_pairs = jnp.concatenate(
        [ctx_keys, ctx_projected[:, kv_width:].astype(jnp.bfloat16)], axis=1
    )
    prefix_mapped = math.log(tok_count / (2.0 * ctx_rows))
    stat_shape = (tok_count, kv_heads, group_size)
    start_state = (
        jnp.full(stat_shape, -jnp.inf, jnp.float32),
        jnp.zeros(stat_shape, jnp.float32),
        jnp.zeros(stat_shape + (CHANNEL_SPAN,), jnp.float32),
    )
    ctx_whole = lax.all_gather(ctx_pairs, "sp", axis=0, tiled=True)
    ctx_state = group_walker(
        start_state,
        probe_entries,
        ctx_whole,
        jnp.full((ctx_whole.shape[0],), prefix_mapped, jnp.float32),
    )
    key_piece = lax.all_gather(own_pairs, "sp", axis=0, tiled=True)
    final_state = group_walker(
        ctx_state, probe_entries, key_piece, jnp.zeros((key_piece.shape[0],), jnp.float32)
    )
    row_peak, row_total, weighted = final_state
    attended = (weighted / row_total[..., None]).astype(jnp.bfloat16).reshape(tok_count, q_width)
    branch = jnp.dot(
        lax.all_to_all(attended, "tp", split_axis=0, concat_axis=1, tiled=True),
        output_weight,
        preferred_element_type=jnp.float32,
    )
    return (latent.astype(jnp.float32) + gates[0] * branch).astype(jnp.bfloat16)


def solution(mesh):
    in_specs = (
        P(("sp", "tp"), None),
        P("sp", None),
        P(),
        P(),
        P(),
        P("sp", "tp"),
        P("sp", "tp"),
        P("sp", "tp"),
        P(None, "tp"),
        P(None, "tp"),
        P(None, "tp"),
        P(),
        P(),
        P(),
    )
    out_specs = P(("sp", "tp"), None)
    return jax.shard_map(
        on_device, mesh=mesh, in_specs=in_specs, out_specs=out_specs, check_vma=False
    )
```

profile of v0, /device:TPU:0, one launch (start us, length us, event | category | flops | bytes accessed | tf_op | source)
XLA Modules:
  0.0 205.1 jit_solution(11449940155735415239)
XLA Ops:
  6.5 1.3 fusion.31
  7.8 0.9 convolution_dynamic-update-slice_fusion.1
  8.8 1.2 convolution_dynamic-update-slice_fusion
  10.0 1.2 convolution_dynamic-update-slice_fusion.2
  11.2 42.4 %all-reduce = (f32[2,2048]{1,0:T(2,128)S(1)}, f32[2,2048]{1,0:T(2,128)S(1)}, f32[2,2048]{1,0:T(2,128)S(1)}) all-reduce(f32[2,2048]{1,0:T(2,128)S(1)} %convolution_dynamic-update-slice_fusion, f32[2,2048]{1,0:T(2,128)S(1)} %convolution_dynamic-update-slice_fusion.1, ...), channel_id=1, replica_groups=mesh['sp'=8,'tp'=4] {'sp','tp'}, use_global_device_ids=true, to_apply=%region_3.4 | all-reduce | flops 12288 | bytes 98304 | tf_op jit(solution)/shard_map/psum | solution.py:137
  53.6 2.1 %fusion.35 = bf16[128,2048]{1,0:T(8,128)(2,1)} fusion(bf16[128,2048]{1,0:T(8,128)(2,1)} %param.16, f32[2048]{0:T(1024)S(1)} %bitcast.136, f32[2048]{0:T(1024)S(1)} %bitcast.135, f32[2048]{0:T(1024)} %param.20, f32[128]{0:T(128)S(1)} %add_rsqrt_fusion.3), kind=kLoop, calls=%fused_computation.40 | loop fusion | flops 1572864 | bytes 1073664 | tf_op jit(solution)/shard_map/convert_element_type | solution.py:19
  56.9 1.1 fusion.40
  58.1 20.3 %all-gather.3.cloned.1.call-done = bf16[512,2048]{1,0:T(8,128)(2,1)} async-done(((bf16[128,2048]{1,0:T(8,128)(2,1)}), bf16[512,2048]{1,0:T(8,128)(2,1)}) %all-gather.3.cloned.1.call-update) | async-done | bytes 2097168 | tf_op jit(solution)/shard_map/all_gather | solution.py:152
  78.3 3.5 %fusion.17 = f32[512,512]{0,1:T(8,128)S(1)} fusion(bf16[512,2048]{1,0:T(8,128)(2,1)} %all-gather.3.cloned.1.call-done, bf16[2048,128]{1,0:T(8,128)(2,1)} %param.26, bf16[2048,128]{1,0:T(8,128)(2,1)} %param.25, bf16[2048,256]{1,0:T(8,128)(2,1)} %param.24), kind=kOutput, calls=%fused_computation.22 | convolution fusion | flops 1080033280 | bytes 5242880 | tf_op jit(solution)/shard_map/dot_general | solution.py:151
  84.0 31.9 %all_gather.9 = bf16[512,256]{1,0:T(8,128)(2,1)S(1)} all-gather(bf16[64,256]{1,0:T(8,128)(2,1)S(1)} %pad_maximum_fusion.4), channel_id=1, replica_groups=mesh['sp'=8,'tp'=4] {'sp'}, dimensions={0}, use_global_device_ids=true | all-gather | bytes 294912 | tf_op jit(solution)/shard_map/all_gather | solution.py:184
  117.2 0.8 fusion.14
  118.1 1.0 fusion.28
  119.1 15.0 %all-gather.5.cloned.1.call-done = bf16[4096,256]{0,1:T(8,128)(2,1)} async-done(((bf16[512,256]{0,1:T(8,128)(2,1)}), bf16[4096,256]{0,1:T(8,128)(2,1)}) %all-gather.5.cloned.1.call-update) | async-done | bytes 2097168 | tf_op jit(solution)/shard_map/all_gather | solution.py:191
  134.1 1.7 copy.61
  135.8 48.4 %while.14 = (s32[]{:T(128)}, f32[512,2,2]{0,2,1:T(2,128)S(1)}, f32[512,2,2]{0,2,1:T(2,128)S(1)}, f32[512,2,2,64]{0,3,2,1:T(8,128)S(1)}, bf16[2,2048,256]{1,2,0:T...) while((s32[]{:T(128)}, f32[512,2,2]{0,2,1:T(2,128)S(1)}, f32[512,2,2]{0,2,1:T(2,128)S(1)}, ...), condition=%wide.region_13.14_spmd, body=%wide.region_10.13_spmd.sunk | while | flops 1107562496 | bytes 57016408 | solution.py:91
  136.0 8.1 %bitcast_reduce_fusion.5 = (f32[512,2,2]{0,2,1:T(2,128)S(1)}, f32[2,2048,512,2]{2,1,3,0:T(8,128)}) fusion(bf16[2048,2,64,1]{0,2,3,1:T(8,128)(2,1)S(1)} %bitcast.116, bf16[512,2,2,64]{0,3,2,1:T(8,128)(2,1)S(1)} %get-tuple-element.187), kind=kOutput, calls=%fused_computation.1.clone.1 | convolution fusion | flops 545257472 | bytes 17571840 | tf_op jit(solution)/shard_map/while/body/eval_jaxpr/dmvk,hmk->dmvh/dot_general | solution.py:58
  144.1 8.5 %fusion.94 = f32[512,2,2]{0,2,1:T(2,128)S(1)} fusion(f32[2,2048,512,2]{2,1,3,0:T(8,128)} %get-tuple-element.164, f32[512,2,2]{0,2,1:T(2,128)S(1)} %max.4), kind=kLoop, calls=%fused_computation.4.clone.1 | loop fusion | flops 12580864 | bytes 16793600 | tf_op jit(solution)/shard_map/while/body/eval_jaxpr/reduce_sum | solution.py:67
  152.6 7.3 %fusion.95 = f32[512,2,2,64]{0,3,2,1:T(8,128)S(1)} fusion(bf16[2048,2,64,1]{0,2,3,1:T(8,128)(2,1)S(1)} %bitcast.117, f32[2,2048,512,2]{2,1,3,0:T(8,128)} %get-tuple-element.164, f32[512,2,2]{0,2,1:T(2,128)S(1)} %max.4, f32[512,2,2,64]{0,3,2,1:T(8,128)S(1)} %get-tuple-element.178, f32[512,2,2]{0,2,1:T(2,128)S(1)} %get-tuple-element.167), kind=kOutput, calls=%fused_computation.7.clone.1 | convolution fusion | flops 549715968 | bytes 18366464 | tf_op jit(solution)/shard_map/while/body/eval_jaxpr/qkgn,nkd->qkgd/dot_general | solution.py:68
  160.2 8.1 %bitcast_reduce_fusion.5 = (f32[512,2,2]{0,2,1:T(2,128)S(1)}, f32[2,2048,512,2]{2,1,3,0:T(8,128)}) fusion(bf16[2048,2,64,1]{0,2,3,1:T(8,128)(2,1)S(1)} %bitcast.116, bf16[512,2,2,64]{0,3,2,1:T(8,128)(2,1)S(1)} %get-tuple-element.187), kind=kOutput, calls=%fused_computation.1.clone.1 | convolution fusion | flops 545257472 | bytes 17571840 | tf_op jit(solution)/shard_map/while/body/eval_jaxpr/dmvk,hmk->dmvh/dot_general | solution.py:58
  168.3 8.5 %fusion.94 = f32[512,2,2]{0,2,1:T(2,128)S(1)} fusion(f32[2,2048,512,2]{2,1,3,0:T(8,128)} %get-tuple-element.164, f32[512,2,2]{0,2,1:T(2,128)S(1)} %max.4), kind=kLoop, calls=%fused_computation.4.clone.1 | loop fusion | flops 12580864 | bytes 16793600 | tf_op jit(solution)/shard_map/while/body/eval_jaxpr/reduce_sum | solution.py:67
  176.9 7.3 %fusion.95 = f32[512,2,2,64]{0,3,2,1:T(8,128)S(1)} fusion(bf16[2048,2,64,1]{0,2,3,1:T(8,128)(2,1)S(1)} %bitcast.117, f32[2,2048,512,2]{2,1,3,0:T(8,128)} %get-tuple-element.164, f32[512,2,2]{0,2,1:T(2,128)S(1)} %max.4, f32[512,2,2,64]{0,3,2,1:T(8,128)S(1)} %get-tuple-element.178, f32[512,2,2]{0,2,1:T(2,128)S(1)} %get-tuple-element.167), kind=kOutput, calls=%fused_computation.7.clone.1 | convolution fusion | flops 549715968 | bytes 18366464 | tf_op jit(solution)/shard_map/while/body/eval_jaxpr/qkgn,nkd->qkgd/dot_general | solution.py:68
  185.1 3.4 %all-to-all-start = ((bf16[4,128,256]{1,2,0:T(8,128)(2,1)}), bf16[4,128,256]{1,2,0:T(8,128)(2,1)S(1)}, u32[]{:S(2)}, u32[]{:S(2)}) async-start(bf16[4,128,256]{1,2,0:T(8,128)(2,1)} %copy.51), calls=%async_computation | async-start | bytes 524288 | tf_op jit(solution)/shard_map/all_to_all | solution.py:198
  188.5 6.0 %all-to-all-done = bf16[4,128,256]{1,2,0:T(8,128)(2,1)S(1)} async-done(((bf16[4,128,256]{1,2,0:T(8,128)(2,1)}), bf16[4,128,256]{1,2,0:T(8,128)(2,1)S(1)}, u32[]{:S(2)}, u32[]{:S(2)}) %all-to-all-start) | async-done | bytes 262176 | tf_op jit(solution)/shard_map/all_to_all | solution.py:198
  194.5 3.8 %fusion.16 = bf16[128,2048]{1,0:T(8,128)(2,1)} fusion(bf16[128,1024]{0,1:T(8,128)(2,1)S(1)} %bitcast.124, bf16[1024,2048]{1,0:T(8,128)(2,1)} %param.29, bf16[128,2048]{1,0:T(8,128)(2,1)} %param.16, f32[2048]{0:T(1024)S(1)} %bitcast.134), kind=kOutput, calls=%fused_computation.20 | convolution fusion | flops 537919488 | bytes 5513216 | tf_op jit(solution)/shard_map/dot_general | solution.py:197
  (75 shorter events, 5.9 us)
Async XLA Ops:
  6.5 1.3 copy-start
  6.5 71.8 %all-gather.3.cloned.1.call-start = ((), (), s32[]{:S(2)}) async-start(), calls=%async_computation.1 | async-start | bytes 2621440 | tf_op jit(solution)/shard_map/all_gather | solution.py:152
  55.8 78.3 %all-gather.5.cloned.1.call-start = ((), (), s32[]{:S(2)}) async-start(), calls=%async_computation.2 | async-start | bytes 2359296 | tf_op jit(solution)/shard_map/all_gather | solution.py:191
  58.0 24.8 %copy-start.3 = (f32[64]{0:T(128)S(1)}, f32[64]{0:T(128)}, u32[]{:S(2)}) copy-start(f32[64]{0:T(128)} %param.28) | copy-start | bytes 772
  58.0 24.9 %copy-start.4 = (f32[64]{0:T(128)S(1)}, f32[64]{0:T(128)}, u32[]{:S(2)}) copy-start(f32[64]{0:T(128)} %param.27) | copy-start | bytes 772
  58.0 25.0 %copy-start.1 = (bf16[64,2048]{1,0:T(8,128)(2,1)S(1)}, bf16[64,2048]{1,0:T(8,128)(2,1)}, u32[]{:S(2)}) copy-start(bf16[64,2048]{1,0:T(8,128)(2,1)} %param.17) | copy-start | bytes 786436
  58.1 25.0 %copy-start.2 = (f32[2048]{0:T(1024)S(1)}, f32[2048]{0:T(1024)}, u32[]{:S(2)}) copy-start(f32[2048]{0:T(1024)} %param.20) | copy-start | bytes 24580
  58.1 25.0 %copy-start.5 = (bf16[2048,128]{1,0:T(8,128)(2,1)S(1)}, bf16[2048,128]{1,0:T(8,128)(2,1)}, u32[]{:S(2)}) copy-start(bf16[2048,128]{1,0:T(8,128)(2,1)} %param.26) | copy-start | bytes 1572868
  58.1 25.0 %copy-start.6 = (bf16[2048,128]{1,0:T(8,128)(2,1)S(1)}, bf16[2048,128]{1,0:T(8,128)(2,1)}, u32[]{:S(2)}) copy-start(bf16[2048,128]{1,0:T(8,128)(2,1)} %param.25) | copy-start | bytes 1572868
  185.1 9.4 %all-to-all-start = ((bf16[4,128,256]{1,2,0:T(8,128)(2,1)}), bf16[4,128,256]{1,2,0:T(8,128)(2,1)S(1)}, u32[]{:S(2)}, u32[]{:S(2)}) async-start(bf16[4,128,256]{1,2,0:T(8,128)(2,1)} %copy.51), calls=%async_computation | async-start | bytes 524288 | tf_op jit(solution)/shard_map/all_to_all | solution.py:198
Sparse Core Ops, SparseCore 0:
  55.9 22.4 all-gather.2
  83.0 51.0 all-gather.4
where the time goes:
time: 206 us; the launch traced here: 205 us
  blocking collectives  74.3 us (36%)
  matrix products  43.6 us (21%)
  waiting for transfers between devices  41.2 us (20%)
  other arithmetic  24.3 us (12%)
  between operations  13.8 us (7%)
  local copies, waits for them, and re-layouts  4.5 us (2%)
  starting transfers between devices  3.45 us (2%)
    psum x1, blocking collectives, on_device(): lax.psum((widen(part_shift), widen(part_scale), widen(part_gate)), ('sp',...  42.4 us
    all_gather x1, blocking collectives, on_device(): ctx_whole = lax.all_gather(ctx_pairs, 'sp', axis=0, tiled=True)  31.9 us
    all_gather x1, waiting for transfers between devices, on_device(): lax.all_gather(hidden, 'tp', axis=0, tiled=True)  20.3 us
    reduce_sum x3, other arithmetic, process_probe_group(): row_total = row_total * shrink + jnp.sum(shares, axis=-1)  17.9 us
    dot_general x3, matrix products, process_probe_group(): jnp.einsum('dmvk,hmk->dmvh', probe_entries, matcher_pieces, preferred_ele...  17 us
    dot_general x3, matrix products, process_probe_group(): jnp.einsum('qkgn,nkd->qkgd', shares.astype(jnp.bfloat16), value_rows, pre...  15.7 us
    all_gather x1, waiting for transfers between devices, on_device(): key_piece = lax.all_gather(own_pairs, 'sp', axis=0, tiled=True)  15 us
    all_to_all x1, waiting for transfers between devices, on_device(): lax.all_to_all(attended, 'tp', split_axis=0, concat_axis=1, tiled=True)  5.96 us
  transfers between devices with their start and end apart: 3, of which 3 were waited for; matrix products, arithmetic and copies ran while one was open for 3% of the time, Pallas kernels for 0%

commit v1 on v0

v1 whole, which is shorter than its diff:
```python
import functools
import math

import jax
import jax.numpy as jnp
from jax import lax
from jax.experimental import pallas as pl
from jax.experimental.pallas import tpu as pltpu
from jax.sharding import PartitionSpec as P

CHANNEL_SPAN = 64
GRID_W = 64
MESH = pl.DeviceIdType.MESH
VMEM = pl.BlockSpec(memory_space=pltpu.VMEM)
F32 = jnp.float32
BF16 = jnp.bfloat16

epsilon = 1e-06
rope_base = 10000.0


def greet(n_sp, n_tp):
    sp, tp = lax.axis_index("sp"), lax.axis_index("tp")
    barrier = pltpu.get_barrier_semaphore()
    for d in range(1, n_sp):
        pl.semaphore_signal(
            barrier, inc=1, device_id=(lax.rem(sp + d, n_sp), tp), device_id_type=MESH
        )
    for d in range(1, n_tp):
        pl.semaphore_signal(
            barrier, inc=1, device_id=(sp, lax.rem(tp + d, n_tp)), device_id_type=MESH
        )
    pl.semaphore_wait(barrier, n_sp + n_tp - 2)


def gather_kernel(
    n_sp, n_tp, latent, act, w_shift, w_scale, w_gate, lat_all, mods,
    part, parts, lat_send, lat_recv, sp_send, sp_recv, tp_send, tp_recv, own_sem,
):
    sp, tp = lax.axis_index("sp"), lax.axis_index("tp")
    part[...] = jnp.zeros_like(part)
    for i, w in enumerate((w_shift, w_scale, w_gate)):
        part[2 * i : 2 * i + 2, :] = jnp.dot(act[...], w[...], preferred_element_type=F32)[0:2]
    greet(n_sp, n_tp)
    sp_copies = []
    for d in range(1, n_sp):
        c = pltpu.make_async_remote_copy(
            src_ref=part, dst_ref=parts.at[sp], send_sem=sp_send.at[d - 1],
            recv_sem=sp_recv.at[d - 1], device_id=(lax.rem(sp + d, n_sp), tp), device_id_type=MESH,
        )
        c.start()
        sp_copies.append(c)
    lat_copies = []
    for d in range(1, n_tp):
        c = pltpu.make_async_remote_copy(
            src_ref=latent, dst_ref=lat_all.at[tp], send_sem=lat_send.at[d - 1],
            recv_sem=lat_recv.at[d - 1], device_id=(sp, lax.rem(tp + d, n_tp)), device_id_type=MESH,
        )
        c.start()
        lat_copies.append(c)
    own = pltpu.make_async_copy(latent, lat_all.at[tp], own_sem)
    own.start()
    parts[sp] = part[...]
    for c in sp_copies:
        c.wait()
    total = parts[0]
    for j in range(1, n_sp):
        total = total + parts[j]
    part[...] = total
    mods[tp] = total
    tp_copies = []
    for d in range(1, n_tp):
        c = pltpu.make_async_remote_copy(
            src_ref=part, dst_ref=mods.at[tp], send_sem=tp_send.at[d - 1],
            recv_sem=tp_recv.at[d - 1], device_id=(sp, lax.rem(tp + d, n_tp)), device_id_type=MESH,
        )
        c.start()
        tp_copies.append(c)
    own.wait()
    for c in tp_copies + lat_copies:
        c.wait()


def project_kernel(
    n_tp, lat_all, context, mods, norm_gain, w_q, w_k, w_v, q_gain, k_gain, cosine, sine,
    q_out, ctx_out, kv_out, hidden,
):
    own_rows = lat_all.shape[1]
    ctx_rows = context.shape[0]
    q_width = w_q.shape[1]
    kv_width = w_k.shape[1]
    kv_heads = kv_width // CHANNEL_SPAN
    q_heads = q_width // CHANNEL_SPAN
    group = q_heads // kv_heads
    span = mods.shape[2]

    def modulate(read, rows, row):
        total = jnp.zeros((rows, 1), F32)
        for t in range(n_tp):
            x = read(t).astype(F32)
            total = total + jnp.sum(x * x, axis=-1, keepdims=True)
        inv = lax.rsqrt(total / (n_tp * span) + epsilon)
        for t in range(n_tp):
            cols = slice(t * span, (t + 1) * span)
            x = read(t).astype(F32)
            y = x * inv * norm_gain[:, cols] * (1.0 + mods[t, 2 + row : 3 + row, :]) + mods[
                t, row : row + 1, :
            ]
            hidden[0:rows, cols] = y.astype(BF16)

    def headnorm(x, gain):
        width = x.shape[1]
        head = lax.broadcasted_iota(jnp.int32, x.shape, 1) // CHANNEL_SPAN
        sq = x * x
        scale = jnp.zeros_like(x)
        for h in range(width // CHANNEL_SPAN):
            s = jnp.sum(jnp.where(head == h, sq, 0.0), axis=-1, keepdims=True)
            scale = jnp.where(head == h, lax.rsqrt(s / CHANNEL_SPAN + epsilon), scale)
        return x * scale * gain

    def rotate(x, cos, sin):
        width = x.shape[1]
        full = x if width == 128 else jnp.concatenate([x, x], axis=1)
        lane = lax.broadcasted_iota(jnp.int32, full.shape, 1)
        other = jnp.where(lane % 32 < 16, pltpu.roll(full, 112, 1), pltpu.roll(full, 16, 1))
        return (full * cos + other * sin)[:, :width]

    piece = min(128, kv_width)
    modulate(lambda t: context[:, t * span : (t + 1) * span], ctx_rows, 1)
    h = hidden[0:ctx_rows, :]
    k = jnp.dot(h, w_k[...], preferred_element_type=F32)
    for c in range(0, kv_width, piece):
        ctx_out[:, c : c + piece] = headnorm(k[:, c : c + piece], k_gain[:, :piece]).astype(BF16)
    ctx_out[:, kv_width:] = jnp.dot(h, w_v[...], preferred_element_type=F32).astype(BF16)

    def tile(i, carry):
        modulate(lambda t: lat_all[i, :, t * span : (t + 1) * span], own_rows, 0)
        h = hidden[0:own_rows, :]
        rows = pl.ds(pl.multiple_of(i * own_rows, own_rows), own_rows)
        cos, sin = cosine[rows, :], sine[rows, :]
        k = jnp.dot(h, w_k[...], preferred_element_type=F32)
        for c in range(0, kv_width, piece):
            kv_out[rows, c : c + piece] = rotate(
                headnorm(k[:, c : c + piece], k_gain[:, :piece]), cos, sin
            ).astype(BF16)
        kv_out[rows, kv_width:] = jnp.dot(h, w_v[...], preferred_element_type=F32).astype(BF16)
        q = jnp.dot(h, w_q[...], preferred_element_type=F32)
        for c in range(0, q_width, 128):
            y = rotate(headnorm(q[:, c : c + 128], q_gain[...]), cos, sin).astype(BF16)
            y = y.astype(F32) * CHANNEL_SPAN ** (-0.5)
            lane = lax.broadcasted_iota(jnp.int32, y.shape, 1)
            for j in range(2):
                head = c // CHANNEL_SPAN + j
                place = head // group
                moved = y if place % 2 == j else pltpu.roll(y, 64, 1)
                base = place // 2 * 128
                inside = lane // CHANNEL_SPAN == place % 2
                blank = jnp.where(inside, moved, 0.0).astype(BF16)
                for b in range(0, kv_width, piece):
                    q_out[head, rows, b : b + piece] = (
                        blank[:, :piece] if b == base else jnp.zeros((own_rows, piece), BF16)
                    )
        return carry

    lax.fori_loop(0, n_tp, tile, 0)


def attend_kernel(
    n_sp, n_tp, tile_rows, offset, q, ctx, kv, latent, mods, w_out_hbm, out,
    ctx_all, kv_all, peak, total, acc, attended, received, w_out,
    kv_send, kv_recv, ctx_send, ctx_recv, at_send, at_recv, own_sem, w_sem,
):
    sp, tp = lax.axis_index("sp"), lax.axis_index("tp")
    tok, width2 = kv.shape
    width = width2 // 2
    kv_heads = width // CHANNEL_SPAN
    q_heads = q.shape[0]
    group = q_heads // kv_heads
    own_rows = tok // n_tp
    q_width = q_heads * CHANNEL_SPAN
    fetch = pltpu.make_async_copy(w_out_hbm, w_out, w_sem)
    fetch.start()
    greet(n_sp, n_tp)

    def kv_copy(d):
        return pltpu.make_async_remote_copy(
            src_ref=kv, dst_ref=kv_all.at[sp], send_sem=kv_send.at[d - 1],
            recv_sem=kv_recv.at[d - 1], device_id=(lax.rem(sp + d, n_sp), tp), device_id_type=MESH,
        )

    def ctx_copy(d):
        return pltpu.make_async_remote_copy(
            src_ref=ctx, dst_ref=ctx_all.at[sp], send_sem=ctx_send.at[d - 1],
            recv_sem=ctx_recv.at[d - 1], device_id=(lax.rem(sp + d, n_sp), tp), device_id_type=MESH,
        )

    def send(d, carry):
        kv_copy(d).start()
        ctx_copy(d).start()
        return carry

    lax.fori_loop(1, n_sp, send, 0)
    own = pltpu.make_async_copy(ctx, ctx_all.at[sp], own_sem)
    own.start()
    tiles = tok // tile_rows

    def update(keys, values, shift, first):
        def step(i, carry):
            head, r = i // tiles, lax.rem(i, tiles)
            rows = pl.ds(pl.multiple_of(r * tile_rows, tile_rows), tile_rows)
            s = lax.dot_general(
                q[head, rows, :], keys(), (((1,), (1,)), ((), ())), preferred_element_type=F32
            )
            if shift:
                s = s + shift
            top = jnp.max(s, axis=-1, keepdims=True)
            if not first:
                old = peak[head, rows, 0:1]
                top = jnp.maximum(top, old)
                shrink = jnp.exp(old - top)
            e = jnp.exp(s - top)
            row_sum = jnp.sum(e, axis=-1, keepdims=True)
            w = jnp.dot(e.astype(BF16), values(), preferred_element_type=F32)
            if not first:
                row_sum = row_sum + total[head, rows, 0:1] * shrink
                w = w + acc[head, rows, :] * shrink
            peak[head, rows, :] = jnp.broadcast_to(top, (tile_rows, 128))
            total[head, rows, :] = jnp.broadcast_to(row_sum, (tile_rows, 128))
            acc[head, rows, :] = w
            return carry

        lax.fori_loop(0, q_heads * tiles, step, 0)

    update(lambda: kv[:, :width], lambda: kv[:, width:], 0.0, True)

    def block(d, carry):
        kv_copy(d).wait_recv()
        src = lax.rem(sp + n_sp - d, n_sp)
        update(lambda: kv_all[src, :, :width], lambda: kv_all[src, :, width:], 0.0, False)
        return carry

    lax.fori_loop(1, n_sp, block, 0)
    own.wait()

    def ctx_wait(d, carry):
        ctx_copy(d).wait()
        kv_copy(d).wait_send()
        return carry

    lax.fori_loop(1, n_sp, ctx_wait, 0)
    ctx_count = n_sp * ctx.shape[0]
    update(
        lambda: ctx_all[:, :, :width].reshape(ctx_count, width),
        lambda: ctx_all[:, :, width:].reshape(ctx_count, width),
        offset,
        False,
    )
    for t in range(n_tp):
        rows = slice(t * own_rows, (t + 1) * own_rows)
        for h in range(q_heads):
            g = h // group
            a = acc[h, rows, :] / total[h, rows, 0:1]
            attended[t, :, h * CHANNEL_SPAN : (h + 1) * CHANNEL_SPAN] = a[
                :, g * CHANNEL_SPAN : (g + 1) * CHANNEL_SPAN
            ].astype(BF16)
    copies = []
    for d in range(1, n_tp):
        peer = lax.rem(tp + d, n_tp)
        c = pltpu.make_async_remote_copy(
            src_ref=attended.at[peer], dst_ref=received.at[tp], send_sem=at_send.at[d - 1],
            recv_sem=at_recv.at[d - 1], device_id=(sp, peer), device_id_type=MESH,
        )
        c.start()
        copies.append(c)
    received[tp] = attended[tp]
    fetch.wait()
    for c in copies:
        c.wait()
    span = mods.shape[2]
    for t in range(n_tp):
        cols = slice(t * span, (t + 1) * span)
        branch = jnp.zeros((own_rows, span), F32)
        for s in range(n_tp):
            branch = branch + jnp.dot(
                received[s],
                w_out[s * q_width : (s + 1) * q_width, cols],
                preferred_element_type=F32,
            )
        out[:, cols] = (latent[:, cols].astype(F32) + mods[t, 4:5, :] * branch).astype(BF16)


def on_device(
    latent, context, condition, context_condition, norm_gain, shift_weight, scale_weight,
    gate_weight, query_weight, key_weight, value_weight, query_gain, key_gain, output_weight,
):
    n_sp, n_tp = lax.axis_size("sp"), lax.axis_size("tp")
    seq_index = lax.axis_index("sp")
    row_slab, columns = shift_weight.shape
    own_rows, model = latent.shape
    ctx_rows = context.shape[0]
    tok = own_rows * n_tp
    q_width, kv_width = query_weight.shape[1], key_weight.shape[1]
    q_heads = q_width // CHANNEL_SPAN
    conditions = jnp.stack([condition, context_condition])
    act = jax.nn.silu(
        lax.dynamic_slice_in_dim(conditions, seq_index * row_slab, row_slab, 1)
    ).astype(BF16)
    act = jnp.pad(act, ((0, 14), (0, 0)))
    dma = pltpu.SemaphoreType.DMA
    lat_all, mods = pl.pallas_call(
        functools.partial(gather_kernel, n_sp, n_tp),
        out_shape=(
            jax.ShapeDtypeStruct((n_tp, own_rows, model), BF16),
            jax.ShapeDtypeStruct((n_tp, 8, columns), F32),
        ),
        in_specs=[VMEM] * 5,
        out_specs=(VMEM, VMEM),
        scratch_shapes=[
            pltpu.VMEM((8, columns), F32),
            pltpu.VMEM((n_sp, 8, columns), F32),
            dma((n_tp - 1,)), dma((n_tp - 1,)), dma((n_sp - 1,)), dma((n_sp - 1,)),
            dma((n_tp - 1,)), dma((n_tp - 1,)), dma,
        ],
        compiler_params=pltpu.CompilerParams(
            collective_id=0, has_side_effects=True, vmem_limit_bytes=30 << 20
        ),
        name="gather_rows",
    )(latent, act, shift_weight, scale_weight, gate_weight)

    quarter = CHANNEL_SPAN // 4
    places = seq_index * tok + jnp.arange(tok, dtype=jnp.int32)
    lane = jnp.arange(128, dtype=jnp.int32) % CHANNEL_SPAN
    inverse = rope_base ** (-(lane % quarter).astype(F32) / quarter)
    coord = jnp.where(
        lane[None, :] < 2 * quarter, (places // GRID_W)[:, None], (places % GRID_W)[:, None]
    ).astype(F32)
    angles = coord * inverse
    cosine = jnp.cos(angles)
    sine = jnp.where(lane % (2 * quarter) < quarter, -1.0, 1.0) * jnp.sin(angles)
    q, ctx, kv = pl.pallas_call(
        functools.partial(project_kernel, n_tp),
        out_shape=(
            jax.ShapeDtypeStruct((q_heads, tok, kv_width), BF16),
            jax.ShapeDtypeStruct((ctx_rows, 2 * kv_width), BF16),
            jax.ShapeDtypeStruct((tok, 2 * kv_width), BF16),
        ),
        in_specs=[VMEM] * 11,
        out_specs=(VMEM, VMEM, VMEM),
        scratch_shapes=[pltpu.VMEM((max(own_rows, ctx_rows), model), BF16)],
        compiler_params=pltpu.CompilerParams(vmem_limit_bytes=40 << 20),
        name="project",
    )(
        lat_all, context, mods, norm_gain[None], query_weight, key_weight, value_weight,
        jnp.tile(query_gain, 2)[None], jnp.tile(key_gain, 2)[None], cosine, sine,
    )
    offset = math.log(tok / (2.0 * ctx_rows))
    tile_rows = math.gcd(tok, 256)
    return pl.pallas_call(
        functools.partial(attend_kernel, n_sp, n_tp, tile_rows, offset),
        out_shape=jax.ShapeDtypeStruct(latent.shape, BF16),
        in_specs=[VMEM] * 5 + [pl.BlockSpec(memory_space=pl.ANY)],
        out_specs=VMEM,
        scratch_shapes=[
            pltpu.VMEM((n_sp, ctx_rows, 2 * kv_width), BF16),
            pltpu.VMEM((n_sp, tok, 2 * kv_width), BF16),
            pltpu.VMEM((q_heads, tok, 128), F32),
            pltpu.VMEM((q_heads, tok, 128), F32),
            pltpu.VMEM((q_heads, tok, kv_width), F32),
            pltpu.VMEM((n_tp, own_rows, q_width), BF16),
            pltpu.VMEM((n_tp, own_rows, q_width), BF16),
            pltpu.VMEM(output_weight.shape, BF16),
            dma((n_sp - 1,)), dma((n_sp - 1,)), dma((n_sp - 1,)), dma((n_sp - 1,)),
            dma((n_tp - 1,)), dma((n_tp - 1,)), dma, dma,
        ],
        compiler_params=pltpu.CompilerParams(
            collective_id=1, has_side_effects=True, vmem_limit_bytes=56 << 20
        ),
        name="attend",
    )(q, ctx, kv, latent, mods, output_weight)


def solution(mesh):
    in_specs = (
        P(("sp", "tp"), None), P("sp", None), P(), P(), P(),
        P("sp", "tp"), P("sp", "tp"), P("sp", "tp"),
        P(None, "tp"), P(None, "tp"), P(None, "tp"), P(), P(), P(),
    )
    return jax.shard_map(
        on_device, mesh=mesh, in_specs=in_specs, out_specs=P(("sp", "tp"), None), check_vma=False
    )
```

time: 206 us -> 133 us (0.65)
  the two profiles are of different devices: /device:TPU:0 before, /device:TPU:25 now
where the time goes in v1:
time: 133 us; the launch traced here: 132 us
  Pallas kernels  116 us (87%)
  local copies, waits for them, and re-layouts  14.3 us (11%)
  other arithmetic  1.83 us (1%)
    pallas_call x1, Pallas kernels, on_device(): pl.pallas_call(functools.partial(attend_kernel, n_sp, n_tp, tile_rows, of...  84.3 us
    pallas_call x1, Pallas kernels, on_device(): pl.pallas_call(functools.partial(gather_kernel, n_sp, n_tp), out_shape=(j...  27.2 us
    unnamed x27, local copies, waits for them, and re-layouts  12.8 us
    pallas_call x1, Pallas kernels, on_device(): pl.pallas_call(functools.partial(project_kernel, n_tp), out_shape=(jax.Sh...  4.58 us

profile of v1, /device:TPU:25, one launch (start us, length us, event | category | flops | bytes accessed | tf_op | source)
XLA Modules:
  0.0 132.3 jit_solution(17618114330716090307)
XLA Ops:
  0.0 0.8 fusion.3
  0.8 0.7 tile.4
  1.5 0.1 broadcast_in_dim_tile.6.q_gain
  1.5 0.7 tile.5
  2.2 0.1 broadcast_in_dim_tile.7.k_gain
  2.3 1.0 sine_multiply_fusion
  3.3 0.0 copy-start
  3.4 1.0 copy-done
  4.4 0.9 copy-done.6
  5.3 0.9 copy-done.7
  6.3 0.9 copy-done.8
  7.2 27.2 %gather_rows.1 = (bf16[4,128,2048]{2,1,0:T(8,128)(2,1)S(1)}, f32[4,8,512]{2,1,0:T(8,128)S(1)}) custom-call(bf16[128,2048]{1,0:T(8,128)(2,1)S(1)} %copy-done, bf16[16,256]{1,0:T(8,128)(2,1)S(1)} %pad.4.act, bf16[256,512]{1,0:T(8,128)(2,1)S(1)} %copy-done.6, bf16[256,512]{1,0:T(8,128)(2,1)S(1)} %copy-done.7, bf16[256,512]{1,0:T(8,128)(2,1)S(1)} %copy-done.8), custom_call_target="tpu_custom_call" | custom-call | tf_op jit(solution)/shard_map/gather_rows/pallas_call | solution.py:310
  34.4 0.0 copy-start.1
  34.4 1.2 copy-done.1
  35.7 1.0 copy-done.3
  36.7 1.0 copy-done.4
  37.8 0.9 copy-done.9
  38.7 0.7 copy-done.12
  39.4 4.6 %project.1 = (bf16[4,512,128]{2,1,0:T(8,128)(2,1)S(1)}, bf16[64,256]{1,0:T(8,128)(2,1)S(1)}, bf16[512,256]{1,0:T(8,128)(2,1)S(1)}) custom-call(bf16[4,128,2048]{2,1,0:T(8,128)(2,1)S(1)} %get-tuple-element.10.lat_all, bf16[64,2048]{1,0:T(8,128)(2,1)S(1)} %copy-done.9, f32[4,8,512]{2,1,0:T(8,128)S(1)} %get-tuple-element.11.mods, f32[1,2048]{1,0:T(1,128)S(1)} %bitcast.3, ...), custom_call_target="tpu_custom_call" | custom-call | tf_op jit(solution)/shard_map/project/pallas_call | solution.py:340
  44.0 0.8 copy-done.2
  44.8 0.7 copy-done.10
  45.5 0.6 copy-done.11
  46.1 84.3 %attend.1 = bf16[128,2048]{1,0:T(8,128)(2,1)} custom-call(bf16[4,512,128]{2,1,0:T(8,128)(2,1)} %copy-done.2, bf16[64,256]{1,0:T(8,128)(2,1)} %copy-done.11, bf16[512,256]{1,0:T(8,128)(2,1)} %copy-done.10, bf16[128,2048]{1,0:T(8,128)(2,1)} %latent.3, f32[4,8,512]{2,1,0:T(8,128)} %copy-done.5, bf16[1024,2048]{1,0:T(8,128)(2,1)} %w_out_hbm.1), custom_call_target="tpu_custom_call" | custom-call | tf_op jit(solution)/shard_map/attend/pallas_call | solution.py:358
  130.4 1.9 %copy.16 = bf16[128,2048]{1,0:T(8,128)(2,1)} copy(bf16[128,2048]{1,0:T(8,128)(2,1)} %attend.1) | data formatting | bytes 1048576
  (16 shorter events, 0.1 us)
Async XLA Ops:
  3.3 1.0 copy-start
  4.4 0.9 copy-start.6
  5.3 0.9 copy-start.7
  6.3 0.9 copy-start.8
  34.4 11.7 %copy-start.5 = (f32[4,8,512]{2,1,0:T(8,128)}, f32[4,8,512]{2,1,0:T(8,128)S(1)}, u32[]{:S(2)}) copy-start(f32[4,8,512]{2,1,0:T(8,128)S(1)} %get-tuple-element.11.mods) | copy-start | bytes 196612
  34.4 1.3 copy-start.1
  35.7 1.0 copy-start.3
  36.7 1.0 copy-start.4
  37.8 0.9 copy-start.9
  38.7 0.7 copy-start.12
  44.0 0.8 copy-start.2
  44.8 0.7 copy-start.10
  45.5 0.6 copy-start.11

commit v2 on v1

--- a/solution.py
+++ b/solution.py
@@ -10,6 +10,8 @@
 
 CHANNEL_SPAN = 64
 GRID_W = 64
+TILE = 256
+UNROLL = 2
 MESH = pl.DeviceIdType.MESH
 VMEM = pl.BlockSpec(memory_space=pltpu.VMEM)
 F32 = jnp.float32
@@ -34,14 +36,39 @@
 
 
 def gather_kernel(
-    n_sp, n_tp, latent, act, w_shift, w_scale, w_gate, lat_all, mods,
-    part, parts, lat_send, lat_recv, sp_send, sp_recv, tp_send, tp_recv, own_sem,
+    n_sp, n_tp, latent_hbm, act, w_shift_hbm, w_scale_hbm, w_gate_hbm, context_hbm, norm_gain,
+    w_q_hbm, w_k_hbm, w_v_hbm, q_gain, k_gain, cosine, sine, q_out, kv_out, mods,
+    lat_all, w_mod, context, w_q, w_k, w_v, hidden, part, parts,
+    load, lat_send, lat_recv, fwd_send, sp_send, sp_recv, tp_send, tp_recv,
 ):
     sp, tp = lax.axis_index("sp"), lax.axis_index("tp")
+    loads = [
+        pltpu.make_async_copy(src, dst, load.at[i])
+        for i, (src, dst) in enumerate(
+            (
+                (w_shift_hbm, w_mod.at[0]), (w_scale_hbm, w_mod.at[1]), (w_gate_hbm, w_mod.at[2]),
+                (latent_hbm, lat_all.at[tp]), (context_hbm, context),
+                (w_k_hbm, w_k), (w_v_hbm, w_v), (w_q_hbm, w_q),
+            )
+        )
+    ]
+    for c in loads:
+        c.start()
+    greet(n_sp, n_tp)
+    core = lax.rem(tp, 2)
+    twin = tp + 1 - 2 * core
+    chips = n_tp // 2
+
+    def row_copy(src, send_sem, peer):
+        return pltpu.make_async_remote_copy(
+            src_ref=lat_all.at[src], dst_ref=lat_all.at[src], send_sem=send_sem,
+            recv_sem=lat_recv.at[src], device_id=(sp, peer), device_id_type=MESH,
+        )
+
     part[...] = jnp.zeros_like(part)
-    for i, w in enumerate((w_shift, w_scale, w_gate)):
-        part[2 * i : 2 * i + 2, :] = jnp.dot(act[...], w[...], preferred_element_type=F32)[0:2]
-    greet(n_sp, n_tp)
+    for i in range(3):
+        loads[i].wait()
+        part[2 * i : 2 * i + 2, :] = jnp.dot(act[...], w_mod[i], preferred_element_type=F32)[0:2]
     sp_copies = []
     for d in range(1, n_sp):
         c = pltpu.make_async_remote_copy(
@@ -50,17 +77,14 @@
         )
         c.start()
         sp_copies.append(c)
-    lat_copies = []
-    for d in range(1, n_tp):
-        c = pltpu.make_async_remote_copy(
-            src_ref=latent, dst_ref=lat_all.at[tp], send_sem=lat_send.at[d - 1],
-            recv_sem=lat_recv.at[d - 1], device_id=(sp, lax.rem(tp + d, n_tp)), device_id_type=MESH,
-        )
-        c.start()
-        lat_copies.append(c)
-    own = pltpu.make_async_copy(latent, lat_all.at[tp], own_sem)
-    own.start()
     parts[sp] = part[...]
+    loads[3].wait()
+    sends = []
+    for d in range(1, chips):
+        sends.append(row_copy(tp, lat_send.at[d], lax.rem(tp + 2 * d, n_tp)))
+    sends.append(row_copy(tp, lat_send.at[0], twin))
+    for c in sends:
+        c.start()
     for c in sp_copies:
         c.wait()
     total = parts[0]
@@ -76,14 +100,38 @@
         )
         c.start()
         tp_copies.append(c)
-    own.wait()
-    for c in tp_copies + lat_copies:
+    for c in loads[4:]:
         c.wait()
-
-
-def project_kernel(
+    for c in tp_copies:
+        c.wait()
+    context_step, tile = project(
+        n_tp, lat_all, context, mods, norm_gain, w_q, w_k, w_v, q_gain, k_gain, cosine, sine,
+        q_out, kv_out, hidden,
+    )
+    context_step()
+    tile(tp)
+    forwards = []
+    for d in range(1, chips):
+        src = lax.rem(tp - 2 * d + n_tp, n_tp)
+        row_copy(src, lat_send.at[0], twin).wait_recv()
+        c = row_copy(src, fwd_send.at[d - 1], twin)
+        c.start()
+        forwards.append(c)
+    row_copy(twin, lat_send.at[0], twin).wait_recv()
+    tile(twin)
+    for d in range(1, chips):
+        tile(lax.rem(tp - 2 * d + n_tp, n_tp))
+    for d in range(1, chips):
+        src = lax.rem(twin - 2 * d + n_tp, n_tp)
+        row_copy(src, lat_send.at[0], twin).wait_recv()
+        tile(src)
+    for c in sends + forwards:
+        c.wait_send()
+
+
+def project(
     n_tp, lat_all, context, mods, norm_gain, w_q, w_k, w_v, q_gain, k_gain, cosine, sine,
-    q_out, ctx_out, kv_out, hidden,
+    q_out, kv_out, hidden,
 ):
     own_rows = lat_all.shape[1]
     ctx_rows = context.shape[0]
@@ -126,24 +174,31 @@
         return (full * cos + other * sin)[:, :width]
 
     piece = min(128, kv_width)
-    modulate(lambda t: context[:, t * span : (t + 1) * span], ctx_rows, 1)
-    h = hidden[0:ctx_rows, :]
-    k = jnp.dot(h, w_k[...], preferred_element_type=F32)
-    for c in range(0, kv_width, piece):
-        ctx_out[:, c : c + piece] = headnorm(k[:, c : c + piece], k_gain[:, :piece]).astype(BF16)
-    ctx_out[:, kv_width:] = jnp.dot(h, w_v[...], preferred_element_type=F32).astype(BF16)
-
-    def tile(i, carry):
+
+    def context_step():
+        modulate(lambda t: context[:, t * span : (t + 1) * span], ctx_rows, 1)
+        h = hidden[0:ctx_rows, :]
+        k = jnp.dot(h, w_k[...], preferred_element_type=F32)
+        for c in range(0, kv_width, piece):
+            kv_out[0:ctx_rows, c : c + piece] = headnorm(
+                k[:, c : c + piece], k_gain[:, :piece]
+            ).astype(BF16)
+        kv_out[0:ctx_rows, kv_width:] = jnp.dot(h, w_v[...], preferred_element_type=F32).astype(
+            BF16
+        )
+
+    def tile(i):
         modulate(lambda t: lat_all[i, :, t * span : (t + 1) * span], own_rows, 0)
         h = hidden[0:own_rows, :]
         rows = pl.ds(pl.multiple_of(i * own_rows, own_rows), own_rows)
         cos, sin = cosine[rows, :], sine[rows, :]
+        low = pl.ds(pl.multiple_of(ctx_rows + i * own_rows, 16), own_rows)
         k = jnp.dot(h, w_k[...], preferred_element_type=F32)
         for c in range(0, kv_width, piece):
-            kv_out[rows, c : c + piece] = rotate(
+            kv_out[low, c : c + piece] = rotate(
                 headnorm(k[:, c : c + piece], k_gain[:, :piece]), cos, sin
             ).astype(BF16)
-        kv_out[rows, kv_width:] = jnp.dot(h, w_v[...], preferred_element_type=F32).astype(BF16)
+        kv_out[low, kv_width:] = jnp.dot(h, w_v[...], preferred_element_type=F32).astype(BF16)
         q = jnp.dot(h, w_q[...], preferred_element_type=F32)
         for c in range(0, q_width, 128):
             y = rotate(headnorm(q[:, c : c + 128], q_gain[...]), cos, sin).astype(BF16)
@@ -160,18 +215,17 @@
                     q_out[head, rows, b : b + piece] = (
                         blank[:, :piece] if b == base else jnp.zeros((own_rows, piece), BF16)
                     )
-        return carry
-
-    lax.fori_loop(0, n_tp, tile, 0)
+
+    return context_step, tile
 
 
 def attend_kernel(
-    n_sp, n_tp, tile_rows, offset, q, ctx, kv, latent, mods, w_out_hbm, out,
-    ctx_all, kv_all, peak, total, acc, attended, received, w_out,
-    kv_send, kv_recv, ctx_send, ctx_recv, at_send, at_recv, own_sem, w_sem,
+    n_sp, n_tp, lows, tile_rows, unroll, ctx_rows, offset, q, kv, mods, latent_hbm, w_out_hbm, out,
+    kv_all, peak, total, acc, attended, received, latent, w_out,
+    lo_send, hi_send, fwd_send, kv_recv, at_send, at_recv, own_sem, lat_sem, w_sem,
 ):
     sp, tp = lax.axis_index("sp"), lax.axis_index("tp")
-    tok, width2 = kv.shape
+    tok, width2 = q.shape[1], kv.shape[1]
     width = width2 // 2
     kv_heads = width // CHANNEL_SPAN
     q_heads = q.shape[0]
@@ -179,29 +233,31 @@
     own_rows = tok // n_tp
     q_width = q_heads * CHANNEL_SPAN
     fetch = pltpu.make_async_copy(w_out_hbm, w_out, w_sem)
+    fetch_latent = pltpu.make_async_copy(latent_hbm, latent, lat_sem)
+    greet(n_sp, n_tp)
+    highs = n_sp // lows
+    low, high = lax.rem(sp, lows), sp // lows
+
+    def copy(src, slot, send_sem, peer):
+        return pltpu.make_async_remote_copy(
+            src_ref=slot, dst_ref=kv_all.at[src], send_sem=send_sem,
+            recv_sem=kv_recv.at[src], device_id=(peer, tp), device_id_type=MESH,
+        )
+
+    def low_peer(d):
+        return high * lows + lax.rem(low + d, lows)
+
+    def high_peer(d):
+        return lax.rem(high + d, highs) * lows + low
+
+    sends = [copy(sp, kv, lo_send.at[d - 1], low_peer(d)) for d in range(1, lows)]
+    sends += [copy(sp, kv, hi_send.at[d - 1], high_peer(d)) for d in range(1, highs)]
+    for c in sends:
+        c.start()
+    own = pltpu.make_async_copy(kv, kv_all.at[sp], own_sem)
+    own.start()
     fetch.start()
-    greet(n_sp, n_tp)
-
-    def kv_copy(d):
-        return pltpu.make_async_remote_copy(
-            src_ref=kv, dst_ref=kv_all.at[sp], send_sem=kv_send.at[d - 1],
-            recv_sem=kv_recv.at[d - 1], device_id=(lax.rem(sp + d, n_sp), tp), device_id_type=MESH,
-        )
-
-    def ctx_copy(d):
-        return pltpu.make_async_remote_copy(
-            src_ref=ctx, dst_ref=ctx_all.at[sp], send_sem=ctx_send.at[d - 1],
-            recv_sem=ctx_recv.at[d - 1], device_id=(lax.rem(sp + d, n_sp), tp), device_id_type=MESH,
-        )
-
-    def send(d, carry):
-        kv_copy(d).start()
-        ctx_copy(d).start()
-        return carry
-
-    lax.fori_loop(1, n_sp, send, 0)
-    own = pltpu.make_async_copy(ctx, ctx_all.at[sp], own_sem)
-    own.start()
+    fetch_latent.start()
     tiles = tok // tile_rows
 
     def update(keys, values, shift, first):
@@ -229,32 +285,68 @@
             acc[head, rows, :] = w
             return carry
 
-        lax.fori_loop(0, q_heads * tiles, step, 0)
-
-    update(lambda: kv[:, :width], lambda: kv[:, width:], 0.0, True)
-
-    def block(d, carry):
-        kv_copy(d).wait_recv()
-        src = lax.rem(sp + n_sp - d, n_sp)
-        update(lambda: kv_all[src, :, :width], lambda: kv_all[src, :, width:], 0.0, False)
+        lax.fori_loop(0, q_heads * tiles, step, 0, unroll=unroll)
+
+    def attend(src):
+        update(
+            lambda: kv_all[src, ctx_rows:, :width], lambda: kv_all[src, ctx_rows:, width:],
+            0.0, False,
+        )
+
+    def arrive(src):
+        copy(src, kv, lo_send.at[0], low_peer(0)).wait_recv()
+
+    update(lambda: kv[ctx_rows:, :width], lambda: kv[ctx_rows:, width:], 0.0, True)
+
+    def near(d, carry):
+        src = high * lows + lax.rem(low - d + lows, lows)
+        arrive(src)
+        attend(src)
         return carry
 
-    lax.fori_loop(1, n_sp, block, 0)
+    lax.fori_loop(1, lows, near, 0)
+
+    def column(d, carry):
+        row = lax.rem(high - d + highs, highs) * lows
+        src = row + low
+        arrive(src)
+
+        def pass_on(e, inner):
+            copy(
+                src, kv_all.at[src], fwd_send.at[(d - 1) * (lows - 1) + e - 1], low_peer(e)
+            ).start()
+            return inner
+
+        lax.fori_loop(1, lows, pass_on, 0)
+        attend(src)
+        return carry
+
+    lax.fori_loop(1, highs, column, 0)
+
+    def rest(k, carry):
+        d, e = k // (lows - 1) + 1, lax.rem(k, lows - 1) + 1
+        src = lax.rem(high - d + highs, highs) * lows + lax.rem(low - e + lows, lows)
+        arrive(src)
+        attend(src)
+        return carry
+
+    lax.fori_loop(0, (highs - 1) * (lows - 1), rest, 0)
     own.wait()
-
-    def ctx_wait(d, carry):
-        ctx_copy(d).wait()
-        kv_copy(d).wait_send()
-        return carry
-
-    lax.fori_loop(1, n_sp, ctx_wait, 0)
-    ctx_count = n_sp * ctx.shape[0]
+    ctx_count = n_sp * ctx_rows
     update(
-        lambda: ctx_all[:, :, :width].reshape(ctx_count, width),
-        lambda: ctx_all[:, :, width:].reshape(ctx_count, width),
+        lambda: kv_all[:, :ctx_rows, :width].reshape(ctx_count, width),
+        lambda: kv_all[:, :ctx_rows, width:].reshape(ctx_count, width),
         offset,
         False,
     )
+    for c in sends:
+        c.wait_send()
+
+    def sent(k, carry):
+        copy(sp, kv, fwd_send.at[k], low_peer(1)).wait_send()
+        return carry
+
+    lax.fori_loop(0, (highs - 1) * (lows - 1), sent, 0)
     for t in range(n_tp):
         rows = slice(t * own_rows, (t + 1) * own_rows)
         for h in range(q_heads):
@@ -274,6 +366,7 @@
         copies.append(c)
     received[tp] = attended[tp]
     fetch.wait()
+    fetch_latent.wait()
     for c in copies:
         c.wait()
     span = mods.shape[2]
@@ -307,26 +400,6 @@
     ).astype(BF16)
     act = jnp.pad(act, ((0, 14), (0, 0)))
     dma = pltpu.SemaphoreType.DMA
-    lat_all, mods = pl.pallas_call(
-        functools.partial(gather_kernel, n_sp, n_tp),
-        out_shape=(
-            jax.ShapeDtypeStruct((n_tp, own_rows, model), BF16),
-            jax.ShapeDtypeStruct((n_tp, 8, columns), F32),
-        ),
-        in_specs=[VMEM] * 5,
-        out_specs=(VMEM, VMEM),
-        scratch_shapes=[
-            pltpu.VMEM((8, columns), F32),
-            pltpu.VMEM((n_sp, 8, columns), F32),
-            dma((n_tp - 1,)), dma((n_tp - 1,)), dma((n_sp - 1,)), dma((n_sp - 1,)),
-            dma((n_tp - 1,)), dma((n_tp - 1,)), dma,
-        ],
-        compiler_params=pltpu.CompilerParams(
-            collective_id=0, has_side_effects=True, vmem_limit_bytes=30 << 20
-        ),
-        name="gather_rows",
-    )(latent, act, shift_weight, scale_weight, gate_weight)
-
     quarter = CHANNEL_SPAN // 4
     places = seq_index * tok + jnp.arange(tok, dtype=jnp.int32)
     lane = jnp.arange(128, dtype=jnp.int32) % CHANNEL_SPAN
@@ -337,46 +410,66 @@
     angles = coord * inverse
     cosine = jnp.cos(angles)
     sine = jnp.where(lane % (2 * quarter) < quarter, -1.0, 1.0) * jnp.sin(angles)
-    q, ctx, kv = pl.pallas_call(
-        functools.partial(project_kernel, n_tp),
+    anywhere = pl.BlockSpec(memory_space=pl.ANY)
+    q, kv, mods = pl.pallas_call(
+        functools.partial(gather_kernel, n_sp, n_tp),
         out_shape=(
             jax.ShapeDtypeStruct((q_heads, tok, kv_width), BF16),
-            jax.ShapeDtypeStruct((ctx_rows, 2 * kv_width), BF16),
-            jax.ShapeDtypeStruct((tok, 2 * kv_width), BF16),
+            jax.ShapeDtypeStruct((ctx_rows + tok, 2 * kv_width), BF16),
+            jax.ShapeDtypeStruct((n_tp, 8, columns), F32),
         ),
-        in_specs=[VMEM] * 11,
+        in_specs=[anywhere, VMEM] + [anywhere] * 4 + [VMEM] + [anywhere] * 3 + [VMEM] * 4,
         out_specs=(VMEM, VMEM, VMEM),
-        scratch_shapes=[pltpu.VMEM((max(own_rows, ctx_rows), model), BF16)],
-        compiler_params=pltpu.CompilerParams(vmem_limit_bytes=40 << 20),
-        name="project",
+        scratch_shapes=[
+            pltpu.VMEM((n_tp, own_rows, model), BF16),
+            pltpu.VMEM((3, row_slab, columns), BF16),
+            pltpu.VMEM(context.shape, BF16),
+            pltpu.VMEM(query_weight.shape, BF16),
+            pltpu.VMEM(key_weight.shape, BF16),
+            pltpu.VMEM(value_weight.shape, BF16),
+            pltpu.VMEM((max(own_rows, ctx_rows), model), BF16),
+            pltpu.VMEM((8, columns), F32),
+            pltpu.VMEM((n_sp, 8, columns), F32),
+            dma((8,)), dma((n_tp // 2,)), dma((n_tp,)), dma((max(n_tp // 2 - 1, 1),)),
+            dma((n_sp - 1,)), dma((n_sp - 1,)), dma((n_tp - 1,)), dma((n_tp - 1,)),
+        ],
+        compiler_params=pltpu.CompilerParams(
+            collective_id=0, has_side_effects=True, vmem_limit_bytes=56 << 20
+        ),
+        name="gather_project",
     )(
-        lat_all, context, mods, norm_gain[None], query_weight, key_weight, value_weight,
+        latent, act, shift_weight, scale_weight, gate_weight, context, norm_gain[None],
+        query_weight, key_weight, value_weight,
         jnp.tile(query_gain, 2)[None], jnp.tile(key_gain, 2)[None], cosine, sine,
     )
     offset = math.log(tok / (2.0 * ctx_rows))
-    tile_rows = math.gcd(tok, 256)
+    tile_rows = math.gcd(tok, TILE)
+    lows = 2 ** (int(math.log2(n_sp)) // 2)
     return pl.pallas_call(
-        functools.partial(attend_kernel, n_sp, n_tp, tile_rows, offset),
+        functools.partial(
+            attend_kernel, n_sp, n_tp, lows, tile_rows, UNROLL, ctx_rows, offset
+        ),
         out_shape=jax.ShapeDtypeStruct(latent.shape, BF16),
-        in_specs=[VMEM] * 5 + [pl.BlockSpec(memory_space=pl.ANY)],
+        in_specs=[VMEM] * 3 + [anywhere] * 2,
         out_specs=VMEM,
         scratch_shapes=[
-            pltpu.VMEM((n_sp, ctx_rows, 2 * kv_width), BF16),
-            pltpu.VMEM((n_sp, tok, 2 * kv_width), BF16),
+            pltpu.VMEM((n_sp, ctx_rows + tok, 2 * kv_width), BF16),
             pltpu.VMEM((q_heads, tok, 128), F32),
             pltpu.VMEM((q_heads, tok, 128), F32),
             pltpu.VMEM((q_heads, tok, kv_width), F32),
             pltpu.VMEM((n_tp, own_rows, q_width), BF16),
             pltpu.VMEM((n_tp, own_rows, q_width), BF16),
+            pltpu.VMEM(latent.shape, BF16),
             pltpu.VMEM(output_weight.shape, BF16),
-            dma((n_sp - 1,)), dma((n_sp - 1,)), dma((n_sp - 1,)), dma((n_sp - 1,)),
-            dma((n_tp - 1,)), dma((n_tp - 1,)), dma, dma,
+            dma((lows - 1,)), dma((n_sp // lows - 1,)),
+            dma(((n_sp // lows - 1) * (lows - 1),)), dma((n_sp,)),
+            dma((n_tp - 1,)), dma((n_tp - 1,)), dma, dma, dma,
         ],
         compiler_params=pltpu.CompilerParams(
             collective_id=1, has_side_effects=True, vmem_limit_bytes=56 << 20
         ),
         name="attend",
-    )(q, ctx, kv, latent, mods, output_weight)
+    )(q, kv, mods, latent, output_weight)
 
 
 def solution(mesh):

time: 133 us -> 90.4 us (0.68)
  Pallas kernels: 116 us -> 82.5 us
  local copies, waits for them, and re-layouts: 14.3 us -> 5.03 us
    pallas_call x2 -> x1, Pallas kernels: 88.9 us -> 60.1 us  [on_device(): pl.pallas_call(functools.partial(attend_kernel, n_sp, n_tp, lows, tile_ro...]
    unnamed x27 -> x1, local copies, waits for them, and re-layouts: 12.8 us -> 1.88 us
    pallas_call x1, Pallas kernels: 27.2 us -> 22.4 us  [on_device(): pl.pallas_call(functools.partial(gather_kernel, n_sp, n_tp), out_shape=(j...]
where the time goes in v2:
time: 90.4 us; the launch traced here: 90.2 us
  Pallas kernels  82.5 us (91%)
  local copies, waits for them, and re-layouts  5.03 us (6%)
  other arithmetic  2.63 us (3%)
    pallas_call x1, Pallas kernels, on_device(): pl.pallas_call(functools.partial(attend_kernel, n_sp, n_tp, lows, tile_ro...  60.1 us
    pallas_call x1, Pallas kernels, on_device(): pl.pallas_call(functools.partial(gather_kernel, n_sp, n_tp), out_shape=(j...  22.4 us
    unnamed x1, local copies, waits for them, and re-layouts  1.88 us
    mul x1, other arithmetic, on_device(): jnp.where(lane % (2 * quarter) < quarter, -1.0, 1.0) * jnp.sin(angles)  1.82 us

profile of v2, /device:TPU:25, one launch (start us, length us, event | category | flops | bytes accessed | tf_op | source)
XLA Modules:
  0.0 90.2 jit_solution(3377509544602443637)
XLA Ops:
  0.0 0.8 fusion.3
  0.8 0.7 tile.4
  1.5 0.6 broadcast_in_dim_tile.6.q_gain
  2.1 0.7 tile.5
  2.8 0.6 broadcast_in_dim_tile.7.k_gain
  3.4 0.6 pad.4.act
  4.0 1.8 %sine_multiply_fusion = (f32[512,128]{1,0:T(8,128)}, f32[512,128]{1,0:T(8,128)}) fusion(f32[128]{0:T(128)S(1)} %get-tuple-element.13, f32[128]{0:T(128)S(1)} %get-tuple-element.14, s32[512]{0:T(512)S(1)} %get-tuple-element.15, s32[512]{0:T(512)S(1)} %get-tuple-element.16, pred[128]{0:T(512)(128)(4,1)S(1)} %broadcast_compare_fusion), kind=kLoop, calls=%fused_computation | loop fusion | flops 262144 | bytes 529536 | tf_op jit(solution)/shard_map/mul | solution.py:412
  5.8 22.4 %gather_project.1 = (bf16[4,512,128]{2,1,0:T(8,128)(2,1)}, bf16[576,256]{1,0:T(8,128)(2,1)}, f32[4,8,512]{2,1,0:T(8,128)}) custom-call(bf16[128,2048]{1,0:T(8,128)(2,1)} %latent_hbm.3, bf16[16,256]{1,0:T(8,128)(2,1)} %pad.4.act, bf16[256,512]{1,0:T(8,128)(2,1)} %w_shift_hbm.1, bf16[256,512]{1,0:T(8,128)(2,1)} %w_scale_hbm.1, bf16[256,512]{1,0:T(8,128)(2,1)} %w_gate_hbm.1, ...), custom_call_target="tpu_custom_call" | custom-call | tf_op jit(solution)/shard_map/gather_project/pallas_call | solution.py:414
  28.2 60.1 %attend.1 = bf16[128,2048]{1,0:T(8,128)(2,1)} custom-call(bf16[4,512,128]{2,1,0:T(8,128)(2,1)} %get-tuple-element.8.q, bf16[576,256]{1,0:T(8,128)(2,1)} %get-tuple-element.9.kv, f32[4,8,512]{2,1,0:T(8,128)} %get-tuple-element.10.mods, bf16[128,2048]{1,0:T(8,128)(2,1)} %latent_hbm.3, bf16[1024,2048]{1,0:T(8,128)(2,1)} %w_out_hbm.1), custom_call_target="tpu_custom_call" | custom-call | tf_op jit(solution)/shard_map/attend/pallas_call | solution.py:448
  88.3 1.9 %copy.16 = bf16[128,2048]{1,0:T(8,128)(2,1)} copy(bf16[128,2048]{1,0:T(8,128)(2,1)} %attend.1) | data formatting | bytes 1048576
  (3 shorter events, 0.0 us)

commit v3 on v2

--- a/solution.py
+++ b/solution.py
@@ -10,8 +10,8 @@
 
 CHANNEL_SPAN = 64
 GRID_W = 64
-TILE = 256
-UNROLL = 2
+TILE = 512
+UNROLL = 4
 MESH = pl.DeviceIdType.MESH
 VMEM = pl.BlockSpec(memory_space=pltpu.VMEM)
 F32 = jnp.float32
@@ -52,8 +52,10 @@
             )
         )
     ]
-    for c in loads:
-        c.start()
+    loads[3].start()
+    for i, c in enumerate(loads):
+        if i != 3:
+            c.start()
     greet(n_sp, n_tp)
     core = lax.rem(tp, 2)
     twin = tp + 1 - 2 * core
@@ -65,19 +67,6 @@
             recv_sem=lat_recv.at[src], device_id=(sp, peer), device_id_type=MESH,
         )
 
-    part[...] = jnp.zeros_like(part)
-    for i in range(3):
-        loads[i].wait()
-        part[2 * i : 2 * i + 2, :] = jnp.dot(act[...], w_mod[i], preferred_element_type=F32)[0:2]
-    sp_copies = []
-    for d in range(1, n_sp):
-        c = pltpu.make_async_remote_copy(
-            src_ref=part, dst_ref=parts.at[sp], send_sem=sp_send.at[d - 1],
-            recv_sem=sp_recv.at[d - 1], device_id=(lax.rem(sp + d, n_sp), tp), device_id_type=MESH,
-        )
-        c.start()
-        sp_copies.append(c)
-    parts[sp] = part[...]
     loads[3].wait()
     sends = []
     for d in range(1, chips):
@@ -85,6 +74,19 @@
     sends.append(row_copy(tp, lat_send.at[0], twin))
     for c in sends:
         c.start()
+    part[...] = jnp.zeros_like(part)
+    for i in range(3):
+        loads[i].wait()
+        part[2 * i : 2 * i + 2, :] = jnp.dot(act[...], w_mod[i], preferred_element_type=F32)
+    sp_copies = []
+    for d in range(1, n_sp):
+        c = pltpu.make_async_remote_copy(
+            src_ref=part, dst_ref=parts.at[sp], send_sem=sp_send.at[d - 1],
+            recv_sem=sp_recv.at[d - 1], device_id=(lax.rem(sp + d, n_sp), tp), device_id_type=MESH,
+        )
+        c.start()
+        sp_copies.append(c)
+    parts[sp] = part[...]
     for c in sp_copies:
         c.wait()
     total = parts[0]
@@ -174,6 +176,8 @@
         return (full * cos + other * sin)[:, :width]
 
     piece = min(128, kv_width)
+    q_pair = jnp.concatenate([q_gain[...], q_gain[...]], axis=1)
+    k_pair = jnp.concatenate([k_gain[...], k_gain[...]], axis=1)
 
     def context_step():
         modulate(lambda t: context[:, t * span : (t + 1) * span], ctx_rows, 1)
@@ -181,7 +185,7 @@
         k = jnp.dot(h, w_k[...], preferred_element_type=F32)
         for c in range(0, kv_width, piece):
             kv_out[0:ctx_rows, c : c + piece] = headnorm(
-                k[:, c : c + piece], k_gain[:, :piece]
+                k[:, c : c + piece], k_pair[:, :piece]
             ).astype(BF16)
         kv_out[0:ctx_rows, kv_width:] = jnp.dot(h, w_v[...], preferred_element_type=F32).astype(
             BF16
@@ -196,12 +200,12 @@
         k = jnp.dot(h, w_k[...], preferred_element_type=F32)
         for c in range(0, kv_width, piece):
             kv_out[low, c : c + piece] = rotate(
-                headnorm(k[:, c : c + piece], k_gain[:, :piece]), cos, sin
+                headnorm(k[:, c : c + piece], k_pair[:, :piece]), cos, sin
             ).astype(BF16)
         kv_out[low, kv_width:] = jnp.dot(h, w_v[...], preferred_element_type=F32).astype(BF16)
         q = jnp.dot(h, w_q[...], preferred_element_type=F32)
         for c in range(0, q_width, 128):
-            y = rotate(headnorm(q[:, c : c + 128], q_gain[...]), cos, sin).astype(BF16)
+            y = rotate(headnorm(q[:, c : c + 128], q_pair), cos, sin).astype(BF16)
             y = y.astype(F32) * CHANNEL_SPAN ** (-0.5)
             lane = lax.broadcasted_iota(jnp.int32, y.shape, 1)
             for j in range(2):
@@ -275,13 +279,15 @@
                 top = jnp.maximum(top, old)
                 shrink = jnp.exp(old - top)
             e = jnp.exp(s - top)
-            row_sum = jnp.sum(e, axis=-1, keepdims=True)
+            row_sum = e[:, 0:128]
+            for c in range(128, e.shape[1], 128):
+                row_sum = row_sum + e[:, c : c + 128]
             w = jnp.dot(e.astype(BF16), values(), preferred_element_type=F32)
             if not first:
-                row_sum = row_sum + total[head, rows, 0:1] * shrink
+                row_sum = row_sum + total[head, rows, :] * shrink
                 w = w + acc[head, rows, :] * shrink
             peak[head, rows, :] = jnp.broadcast_to(top, (tile_rows, 128))
-            total[head, rows, :] = jnp.broadcast_to(row_sum, (tile_rows, 128))
+            total[head, rows, :] = row_sum
             acc[head, rows, :] = w
             return carry
 
@@ -351,7 +357,7 @@
         rows = slice(t * own_rows, (t + 1) * own_rows)
         for h in range(q_heads):
             g = h // group
-            a = acc[h, rows, :] / total[h, rows, 0:1]
+            a = acc[h, rows, :] / jnp.sum(total[h, rows, :], axis=-1, keepdims=True)
             attended[t, :, h * CHANNEL_SPAN : (h + 1) * CHANNEL_SPAN] = a[
                 :, g * CHANNEL_SPAN : (g + 1) * CHANNEL_SPAN
             ].astype(BF16)
@@ -398,7 +404,6 @@
     act = jax.nn.silu(
         lax.dynamic_slice_in_dim(conditions, seq_index * row_slab, row_slab, 1)
     ).astype(BF16)
-    act = jnp.pad(act, ((0, 14), (0, 0)))
     dma = pltpu.SemaphoreType.DMA
     quarter = CHANNEL_SPAN // 4
     places = seq_index * tok + jnp.arange(tok, dtype=jnp.int32)
@@ -440,7 +445,7 @@
     )(
         latent, act, shift_weight, scale_weight, gate_weight, context, norm_gain[None],
         query_weight, key_weight, value_weight,
-        jnp.tile(query_gain, 2)[None], jnp.tile(key_gain, 2)[None], cosine, sine,
+        query_gain[None], key_gain[None], cosine, sine,
     )
     offset = math.log(tok / (2.0 * ctx_rows))
     tile_rows = math.gcd(tok, TILE)

time: 90.4 us -> 83.8 us (0.927)
  Pallas kernels: 82.5 us -> 78.4 us
  local copies, waits for them, and re-layouts: 5.03 us -> 1.88 us
    pallas_call x1, Pallas kernels: 60.1 us -> 56.6 us  [on_device(): pl.pallas_call(functools.partial(attend_kernel, n_sp, n_tp, lows, tile_ro...]
    another operation x4 -> x0, local copies, waits for them, and re-layouts: 2.55 us -> none  [the longest x2 1.31 us: on_device(): jnp.tile(query_gain, 2)[None]]
where the time goes in v3:
time: 83.8 us; the launch traced here: 83.6 us
  Pallas kernels  78.4 us (94%)
  other arithmetic  3.21 us (4%)
  local copies, waits for them, and re-layouts  1.88 us (2%)
    pallas_call x1, Pallas kernels, on_device(): pl.pallas_call(functools.partial(attend_kernel, n_sp, n_tp, lows, tile_ro...  56.6 us
    pallas_call x1, Pallas kernels, on_device(): pl.pallas_call(functools.partial(gather_kernel, n_sp, n_tp), out_shape=(j...  21.8 us
    unnamed x1, local copies, waits for them, and re-layouts  1.88 us
    mul x1, other arithmetic, on_device(): jnp.where(lane % (2 * quarter) < quarter, -1.0, 1.0) * jnp.sin(angles)  1.85 us

profile of v3, /device:TPU:25, one launch (start us, length us, event | category | flops | bytes accessed | tf_op | source)
XLA Modules:
  0.0 83.6 jit_solution(17038301305010588754)
XLA Ops:
  0.0 1.3 %fusion.3.act = bf16[2,256]{1,0:T(2,128)(2,1)} fusion(s32[]{:T(128)S(6)} %select_n.71, f32[1,2048]{1,0:T(1,128)} %bitcast.6, f32[1,2048]{1,0:T(1,128)} %bitcast.7), kind=kLoop, calls=%fused_computation.15 | loop fusion | flops 3072 | bytes 17412 | tf_op jit(solution)/shard_map/convert_element_type | solution.py:406
  1.4 1.8 %sine_multiply_fusion = (f32[512,128]{1,0:T(8,128)}, f32[512,128]{1,0:T(8,128)}) fusion(f32[128]{0:T(128)S(1)} %get-tuple-element.13, f32[128]{0:T(128)S(1)} %get-tuple-element.14, s32[512]{0:T(512)S(1)} %get-tuple-element.15, s32[512]{0:T(512)S(1)} %get-tuple-element.16, pred[128]{0:T(512)(128)(4,1)S(1)} %broadcast_compare_fusion), kind=kLoop, calls=%fused_computation | loop fusion | flops 262144 | bytes 529536 | tf_op jit(solution)/shard_map/mul | solution.py:417
  3.2 21.8 %gather_project.1 = (bf16[4,512,128]{2,1,0:T(8,128)(2,1)}, bf16[576,256]{1,0:T(8,128)(2,1)}, f32[4,8,512]{2,1,0:T(8,128)}) custom-call(bf16[128,2048]{1,0:T(8,128)(2,1)} %latent_hbm.3, bf16[2,256]{1,0:T(2,128)(2,1)} %fusion.3.act, bf16[256,512]{1,0:T(8,128)(2,1)} %w_shift_hbm.1, bf16[256,512]{1,0:T(8,128)(2,1)} %w_scale_hbm.1, bf16[256,512]{1,0:T(8,128)(2,1)} %w_gate_hbm.1, ...), custom_call_target="tpu_custom_call" | custom-call | tf_op jit(solution)/shard_map/gather_project/pallas_call | solution.py:419
  25.1 56.6 %attend.1 = bf16[128,2048]{1,0:T(8,128)(2,1)} custom-call(bf16[4,512,128]{2,1,0:T(8,128)(2,1)} %get-tuple-element.8.q, bf16[576,256]{1,0:T(8,128)(2,1)} %get-tuple-element.9.kv, f32[4,8,512]{2,1,0:T(8,128)} %get-tuple-element.10.mods, bf16[128,2048]{1,0:T(8,128)(2,1)} %latent_hbm.3, bf16[1024,2048]{1,0:T(8,128)(2,1)} %w_out_hbm.1), custom_call_target="tpu_custom_call" | custom-call | tf_op jit(solution)/shard_map/attend/pallas_call | solution.py:453
  81.7 1.9 %copy.16 = bf16[128,2048]{1,0:T(8,128)(2,1)} copy(bf16[128,2048]{1,0:T(8,128)(2,1)} %attend.1) | data formatting | bytes 1048576
  (3 shorter events, 0.0 us)

commit v4 on v3

--- a/solution.py
+++ b/solution.py
@@ -37,9 +37,9 @@
 
 def gather_kernel(
     n_sp, n_tp, latent_hbm, act, w_shift_hbm, w_scale_hbm, w_gate_hbm, context_hbm, norm_gain,
-    w_q_hbm, w_k_hbm, w_v_hbm, q_gain, k_gain, cosine, sine, q_out, kv_out, mods,
+    w_q_hbm, w_k_hbm, w_v_hbm, q_gain, k_gain, inverse, q_out, kv_out, mods,
     lat_all, w_mod, context, w_q, w_k, w_v, hidden, part, parts,
-    load, lat_send, lat_recv, fwd_send, sp_send, sp_recv, tp_send, tp_recv,
+    cosine, sine, load, lat_send, lat_recv, fwd_send, sp_send, sp_recv, tp_send, tp_recv,
 ):
     sp, tp = lax.axis_index("sp"), lax.axis_index("tp")
     loads = [
@@ -87,6 +87,14 @@
         c.start()
         sp_copies.append(c)
     parts[sp] = part[...]
+    tok = cosine.shape[0]
+    place = sp * tok + lax.broadcasted_iota(jnp.int32, (tok, 128), 0)
+    lane = lax.broadcasted_iota(jnp.int32, (tok, 128), 1) % CHANNEL_SPAN
+    coord = jnp.where(lane < CHANNEL_SPAN // 2, place // GRID_W, place % GRID_W)
+    angles = coord.astype(F32) * inverse[...]
+    cosine[...] = jnp.cos(angles)
+    turn = jnp.sin(angles)
+    sine[...] = jnp.where(lane % (CHANNEL_SPAN // 2) < CHANNEL_SPAN // 4, -turn, turn)
     for c in sp_copies:
         c.wait()
     total = parts[0]
@@ -406,15 +414,8 @@
     ).astype(BF16)
     dma = pltpu.SemaphoreType.DMA
     quarter = CHANNEL_SPAN // 4
-    places = seq_index * tok + jnp.arange(tok, dtype=jnp.int32)
     lane = jnp.arange(128, dtype=jnp.int32) % CHANNEL_SPAN
-    inverse = rope_base ** (-(lane % quarter).astype(F32) / quarter)
-    coord = jnp.where(
-        lane[None, :] < 2 * quarter, (places // GRID_W)[:, None], (places % GRID_W)[:, None]
-    ).astype(F32)
-    angles = coord * inverse
-    cosine = jnp.cos(angles)
-    sine = jnp.where(lane % (2 * quarter) < quarter, -1.0, 1.0) * jnp.sin(angles)
+    inverse = (rope_base ** (-(lane % quarter).astype(F32) / quarter))[None]
     anywhere = pl.BlockSpec(memory_space=pl.ANY)
     q, kv, mods = pl.pallas_call(
         functools.partial(gather_kernel, n_sp, n_tp),
@@ -423,7 +424,7 @@
             jax.ShapeDtypeStruct((ctx_rows + tok, 2 * kv_width), BF16),
             jax.ShapeDtypeStruct((n_tp, 8, columns), F32),
         ),
-        in_specs=[anywhere, VMEM] + [anywhere] * 4 + [VMEM] + [anywhere] * 3 + [VMEM] * 4,
+        in_specs=[anywhere, VMEM] + [anywhere] * 4 + [VMEM] + [anywhere] * 3 + [VMEM] * 3,
         out_specs=(VMEM, VMEM, VMEM),
         scratch_shapes=[
             pltpu.VMEM((n_tp, own_rows, model), BF16),
@@ -435,6 +436,8 @@
             pltpu.VMEM((max(own_rows, ctx_rows), model), BF16),
             pltpu.VMEM((8, columns), F32),
             pltpu.VMEM((n_sp, 8, columns), F32),
+            pltpu.VMEM((tok, 128), F32),
+            pltpu.VMEM((tok, 128), F32),
             dma((8,)), dma((n_tp // 2,)), dma((n_tp,)), dma((max(n_tp // 2 - 1, 1),)),
             dma((n_sp - 1,)), dma((n_sp - 1,)), dma((n_tp - 1,)), dma((n_tp - 1,)),
         ],
@@ -445,7 +448,7 @@
     )(
         latent, act, shift_weight, scale_weight, gate_weight, context, norm_gain[None],
         query_weight, key_weight, value_weight,
-        query_gain[None], key_gain[None], cosine, sine,
+        query_gain[None], key_gain[None], inverse,
     )
     offset = math.log(tok / (2.0 * ctx_rows))
     tile_rows = math.gcd(tok, TILE)

time: 83.8 us -> 82.1 us (0.980)
  other arithmetic: 3.21 us -> 1.86 us
    mul x1 -> x0, other arithmetic: 1.85 us -> none  [on_device(): jnp.where(lane % (2 * quarter) < quarter, -1.0, 1.0) * jnp.sin(angles)]
where the time goes in v4:
time: 82.1 us; the launch traced here: 81.9 us
  Pallas kernels  78.1 us (95%)
  local copies, waits for them, and re-layouts  1.88 us (2%)
  other arithmetic  1.86 us (2%)
    pallas_call x1, Pallas kernels, on_device(): pl.pallas_call(functools.partial(attend_kernel, n_sp, n_tp, lows, tile_ro...  56.6 us
    pallas_call x1, Pallas kernels, on_device(): pl.pallas_call(functools.partial(gather_kernel, n_sp, n_tp), out_shape=(j...  21.5 us
    unnamed x1, local copies, waits for them, and re-layouts  1.88 us

profile of v4, /device:TPU:25, one launch (start us, length us, event | category | flops | bytes accessed | tf_op | source)
XLA Modules:
  0.0 81.9 jit_solution(6193027387454305997)
XLA Ops:
  0.0 1.3 %fusion.1.act = bf16[2,256]{1,0:T(2,128)(2,1)} fusion(s32[]{:T(128)S(6)} %select_n.28, f32[1,2048]{1,0:T(1,128)} %bitcast.6, f32[1,2048]{1,0:T(1,128)} %bitcast.7), kind=kLoop, calls=%fused_computation.6 | loop fusion | flops 3072 | bytes 17412 | tf_op jit(solution)/shard_map/convert_element_type | solution.py:414
  1.4 0.5 fusion.5.inverse
  1.9 21.5 %gather_project.1 = (bf16[4,512,128]{2,1,0:T(8,128)(2,1)}, bf16[576,256]{1,0:T(8,128)(2,1)}, f32[4,8,512]{2,1,0:T(8,128)}) custom-call(bf16[128,2048]{1,0:T(8,128)(2,1)} %latent_hbm.3, bf16[2,256]{1,0:T(2,128)(2,1)} %fusion.1.act, bf16[256,512]{1,0:T(8,128)(2,1)} %w_shift_hbm.1, bf16[256,512]{1,0:T(8,128)(2,1)} %w_scale_hbm.1, bf16[256,512]{1,0:T(8,128)(2,1)} %w_gate_hbm.1, ...), custom_call_target="tpu_custom_call" | custom-call | tf_op jit(solution)/shard_map/gather_project/pallas_call | solution.py:420
  23.3 56.6 %attend.1 = bf16[128,2048]{1,0:T(8,128)(2,1)} custom-call(bf16[4,512,128]{2,1,0:T(8,128)(2,1)} %get-tuple-element.8.q, bf16[576,256]{1,0:T(8,128)(2,1)} %get-tuple-element.9.kv, f32[4,8,512]{2,1,0:T(8,128)} %get-tuple-element.10.mods, bf16[128,2048]{1,0:T(8,128)(2,1)} %latent_hbm.3, bf16[1024,2048]{1,0:T(8,128)(2,1)} %w_out_hbm.1), custom_call_target="tpu_custom_call" | custom-call | tf_op jit(solution)/shard_map/attend/pallas_call | solution.py:456
  80.0 1.9 %copy.16 = bf16[128,2048]{1,0:T(8,128)(2,1)} copy(bf16[128,2048]{1,0:T(8,128)(2,1)} %attend.1) | data formatting | bytes 1048576
